TPU v7x, 32 devices: a whole 2x2x4 slice. The times are simulated.
32 devices in a mesh: sp: 4 (over y, x), tp: 8 (over z, core).
Axes of the slice: x: 2, y: 2, z: 4, core: 2. Of those that a mesh axis runs over, the one named last changes fastest.
Arguments:
- tokens: bfloat16 [2048, 2048], P(('sp', 'tp')), may hold values from -6 to 6
- query_vectors: bfloat16 [2048, 2048], P('sp', 'tp'), may hold values from -8 to 8
- key_vectors: bfloat16 [2048, 2048], P('sp', 'tp'), may hold values from -8 to 8
- value_vectors: bfloat16 [2048, 2048], P('sp', 'tp'), may hold values from -24 to 24
- cum_gate: float32 [2048, 32], P('sp', 'tp'), may hold values from -260 to 0, as said below
- out_weight: bfloat16 [2048, 2048], P('tp'), may hold values from -0.125 to 0.125
- norm_gain: float32 [2048], replicated, may hold values from 0.1 to 1.9
- gate_weight: bfloat16 [4, 2048, 7168], P('sp', None, 'tp'), may hold values from -0.125 to 0.125
- up_weight: bfloat16 [4, 2048, 7168], P('sp', None, 'tp'), may hold values from -0.125 to 0.125
- down_weight: bfloat16 [4, 7168, 2048], P('sp', 'tp'), may hold values from -0.0625 to 0.0625
- expert_ids: int32 [2048, 2], P(('sp', 'tp')), may hold values from 0 to 3, all different within a row; in each aligned block of 64 rows (0 to 63, 64 to 127, ...) at most 48 rows name the same one
- route_weights: float32 [2048, 2], P(('sp', 'tp')), may hold values from 0.2 to 1
Outputs:
- layer_output: bfloat16 [2048, 2048], P(('sp', 'tp'))
Inputs may be any that keep to these rules, and one draw needn't show every extreme that they name: `cum_gate`: along the positions each head's values never rise. `expert_ids`: within the rows of one device no expert is named by more than 48 rows, and in some devices' rows one expert is named by exactly 48; a row names 2 different experts.
All inputs are finite; a program needn't handle non-finite values.
Results may differ from a plain program's by a relative error of at most 0.014.
Values may be sent and summed in bfloat16 or wider, within the bound.
A program may use at most 128 MiB of HBM per device.

v0:
```python
import math
import jax
import jax.numpy as jnp
from jax import lax
from jax.sharding import PartitionSpec as P

NEG_LARGE = -1e30


def shards(
    tokens,
    query_vectors,
    key_vectors,
    value_vectors,
    cum_gate,
    out_weight,
    norm_gain,
    gate_weight,
    up_weight,
    down_weight,
    expert_ids,
    route_weights,
):
    sp_count = lax.axis_size("sp")
    seg_rows = query_vectors.shape[0]
    heads_here = cum_gate.shape[1]
    head_width = query_vectors.shape[1] // heads_here
    score_scale = head_width ** (-0.5)
    offset = lax.axis_index("sp") * seg_rows
    last_query = offset + seg_rows - 1
    query_pos = offset + jnp.arange(seg_rows, dtype=jnp.int32)
    query_heads = query_vectors.reshape(seg_rows, heads_here, head_width)
    query_gate = cum_gate.T
    gate_rows = lax.all_gather(cum_gate, "sp", axis=0, tiled=True)

    def attend_block(carried, key_block, value_block, block_start):
        running_peak, running_total, accumulated = carried
        row_count = key_block.shape[0]
        key_heads = key_block.reshape(row_count, heads_here, head_width)
        value_heads = value_block.reshape(row_count, heads_here, head_width)
        key_gate = lax.dynamic_slice_in_dim(gate_rows, block_start, row_count, 0).T
        scores = (
            jnp.einsum("qhd,khd->hqk", query_heads, key_heads, preferred_element_type=jnp.float32)
            * score_scale
        )
        scores = scores + query_gate[:, :, None] - key_gate[:, None, :]
        key_pos = block_start + jnp.arange(row_count, dtype=jnp.int32)
        visible = (key_pos[None, :] <= query_pos[:, None])[None]
        scores = jnp.where(visible, scores, NEG_LARGE)
        new_peak = jnp.maximum(running_peak, jnp.max(scores, axis=2))
        exponent = jnp.where(visible, jnp.exp(scores - new_peak[:, :, None]), 0.0)
        rescale = jnp.exp(running_peak - new_peak)
        running_total = running_total * rescale + jnp.sum(exponent, axis=2)
        weighted = jnp.einsum(
            "hqk,khd->hqd",
            exponent.astype(jnp.bfloat16),
            value_heads,
            preferred_element_type=jnp.float32,
        )
        accumulated = accumulated * rescale[:, :, None] + weighted
        return (new_peak, running_total, accumulated)

    start_state = (
        jnp.full((heads_here, seg_rows), NEG_LARGE, jnp.float32),
        jnp.zeros((heads_here, seg_rows), jnp.float32),
        jnp.zeros((heads_here, seg_rows, head_width), jnp.float32),
    )
    carried = start_state
    key_piece = lax.all_gather(key_vectors, "sp", axis=0, tiled=True)
    value_piece = lax.all_gather(value_vectors, "sp", axis=0, tiled=True)
    row_count = key_piece.shape[0]
    block_rows = math.gcd(row_count, 1024)
    block_count = row_count // block_rows
    key_stack = key_piece.reshape(block_count, block_rows, key_piece.shape[1])
    value_stack = value_piece.reshape(block_count, block_rows, value_piece.shape[1])

    def step_block(state, inputs):
        key_block, value_block, block_index = inputs
        block_start = block_index * block_rows

        def take_block(inner):
            return attend_block(inner, key_block, value_block, block_start)

        def skip_block(inner):
            return inner

        return (lax.cond(block_start <= last_query, take_block, skip_block, state), None)

    carried, _ = lax.scan(
        step_block, carried, (key_stack, value_stack, jnp.arange(block_count, dtype=jnp.int32))
    )
    final_peak, final_total, accumulated = carried
    attended = (accumulated / final_total[:, :, None]).astype(jnp.bfloat16)
    attended = attended.transpose(1, 0, 2).reshape(seg_rows, heads_here * head_width)
    tok_dev = tokens.shape[0]
    model_width = tokens.shape[1]
    token_rows = lax.all_to_all(attended, "tp", split_axis=0, concat_axis=1, tiled=True)
    projected = jnp.dot(
        token_rows,
        lax.all_gather(out_weight, "tp", axis=0, tiled=True),
        preferred_element_type=jnp.float32,
    )
    stream_wide = (tokens.astype(jnp.float32) + projected).astype(jnp.bfloat16).astype(jnp.float32)
    inverse = lax.rsqrt(jnp.mean(stream_wide * stream_wide, axis=1, keepdims=True) + 1e-05)
    normed = (stream_wide * inverse * norm_gain[None, :]).astype(jnp.bfloat16)
    n_experts = gate_weight.shape[0] * sp_count
    top_count = expert_ids.shape[1]
    capacity = max(2, 3 * tok_dev * top_count // (2 * n_experts))
    flat_ids = expert_ids.reshape(-1)
    hits = (flat_ids[:, None] == jnp.arange(n_experts, dtype=jnp.int32)[None, :]).astype(jnp.int32)
    earlier = jnp.cumsum(hits, axis=0) - hits
    slot_index = flat_ids * capacity + jnp.sum(earlier * hits, axis=1)
    placement_map = (
        jnp.arange(n_experts * capacity, dtype=jnp.int32)[:, None] == slot_index[None, :]
    ).astype(jnp.bfloat16)
    repeated = jnp.repeat(normed, top_count, axis=0)
    dispatch = jnp.dot(placement_map, repeated, preferred_element_type=jnp.float32).astype(
        jnp.bfloat16
    )
    dispatch = dispatch.reshape(n_experts, capacity, model_width)
    arrived = lax.all_to_all(dispatch, "sp", split_axis=0, concat_axis=0, tiled=True)
    row_block = arrived.reshape(-1, model_width)
    rows_in = lax.all_gather(row_block, "tp", axis=0, tiled=True)
    gate_value = jnp.dot(rows_in, gate_weight[0], preferred_element_type=jnp.float32)
    up_value = jnp.dot(rows_in, up_weight[0], preferred_element_type=jnp.float32)
    hidden = (jax.nn.silu(gate_value) * up_value).astype(jnp.bfloat16)
    summed = lax.psum_scatter(
        jnp.dot(hidden, down_weight[0], preferred_element_type=jnp.float32).astype(jnp.bfloat16),
        "tp",
        scatter_dimension=0,
        tiled=True,
    )
    returned = summed.reshape(arrived.shape)
    back = lax.all_to_all(returned, "sp", split_axis=0, concat_axis=0, tiled=True)
    flat_back = back.reshape(n_experts * capacity, model_width)
    picked = flat_back[slot_index].astype(jnp.float32).reshape(tok_dev, top_count, model_width)
    mixture = jnp.sum(picked * route_weights[:, :, None], axis=1)
    return (stream_wide + mixture).astype(jnp.bfloat16)


def solution(mesh):
    in_specs = (
        P(("sp", "tp"), None),
        P("sp", "tp"),
        P("sp", "tp"),
        P("sp", "tp"),
        P("sp", "tp"),
        P("tp", None),
        P(),
        P("sp", None, "tp"),
        P("sp", None, "tp"),
        P("sp", "tp", None),
        P(("sp", "tp"), None),
        P(("sp", "tp"), None),
    )
    out_specs = P(("sp", "tp"), None)
    return jax.shard_map(shards, mesh=mesh, in_specs=in_specs, out_specs=out_specs, check_vma=False)
```

profile of v0, /device:TPU:0, one launch (start us, length us, event | category | flops | bytes accessed | tf_op | source)
XLA Modules:
  0.0 362.4 jit_solution(4247297287543457111)
XLA Ops:
  6.5 0.7 all-gather.5.cloned.1.call-update
  7.3 0.7 all-gather.7.cloned.1.call-update
  8.1 0.7 all-gather.9.cloned.1.call-update
  8.7 1.1 copy.27
  9.8 0.8 copy.32
  10.6 0.1 reshape.138
  10.8 9.8 %all_gather.16 = f32[2048,4]{0,1:T(4,128)S(1)} all-gather(f32[512,4]{0,1:T(4,128)} %param.20), channel_id=1, replica_groups=mesh['sp'=4,'tp'=8] {'sp'}, dimensions={0}, use_global_device_ids=true | all-gather | bytes 40960 | tf_op jit(solution)/shard_map/all_gather | solution.py:34
  20.6 17.9 %all-gather.5.cloned.1.call-done = bf16[2048,256]{1,0:T(8,128)(2,1)} async-done(((bf16[512,256]{1,0:T(8,128)(2,1)}), bf16[2048,256]{1,0:T(8,128)(2,1)}) %all-gather.5.cloned.1.call-update) | async-done | bytes 1048592 | tf_op jit(solution)/shard_map/all_gather | solution.py:69
  38.4 1.5 copy.28
  39.9 26.9 %all-gather.7.cloned.1.call-done = bf16[2048,256]{1,0:T(8,128)(2,1)} async-done(((bf16[512,256]{1,0:T(8,128)(2,1)}), bf16[2048,256]{1,0:T(8,128)(2,1)}) %all-gather.7.cloned.1.call-update) | async-done | bytes 1048592 | tf_op jit(solution)/shard_map/all_gather | solution.py:70
  66.8 1.5 copy.29
  68.4 12.0 %while.15 = (s32[]{:T(128)}, f32[4,512]{1,0:T(4,128)S(1)}, f32[4,512]{1,0:T(4,128)S(1)}, f32[4,512,64]{1,2,0:T(8,128)S(1)}, s32[2]{0:T(128)S(1)}, /*index=5*/s32...) while((s32[]{:T(128)}, f32[4,512]{1,0:T(4,128)S(1)}, ...), condition=%wide.region_5.6_spmd.clone, body=%wide.region_0.5_spmd.clone.sunk | while | flops 577508864 | bytes 31973748 | solution.py:89
  68.4 0.7 dynamic_slice.31
  69.8 9.2 %conditional.3 = ((f32[4,512]{1,0:T(4,128)S(1)}, f32[4,512]{1,0:T(4,128)S(1)}, f32[4,512,64]{1,2,0:T(8,128)S(1)})) conditional(s32[]{:T(128)} %convert_element_type.83, (f32[4,512]{1,0:T(4,128)S(1)}, f32[4,512]{1,0:T(4,128)S(1)}, f32[4,512,64]{1,2,0:T(8,128)S(1)}) %tuple.42, (s32[]{:T(128)}, s32[]{:T(128)}, bf16[2,1024,256]{1,2,0:T(8,128)(2,1)S(1)}, ...), branch_computations={%region_1.1_spmd, %region_2.4_spmd} | conditional | flops 577508864 | bytes 31971410 | solution.py:87
  69.8 0.1 dynamic-slice_bitcast_fusion
  69.9 0.4 broadcast_compare_fusion
  70.3 0.1 constant_dynamic-slice_fusion
  70.4 2.5 fusion.4
  72.9 2.9 fusion.3
  75.8 3.2 fusion.8
  79.0 0.7 dynamic_slice.31
  80.5 0.3 all_to_all.20
  80.8 1.0 copy.30
  81.8 4.6 %all-to-all-start = ((bf16[8,64,256]{2,1,0:T(8,128)(2,1)}), bf16[8,64,256]{2,1,0:T(8,128)(2,1)S(1)}, u32[]{:S(2)}, u32[]{:S(2)}) async-start(bf16[8,64,256]{2,1,0:T(8,128)(2,1)} %copy.30), calls=%async_computation | async-start | bytes 524288 | tf_op jit(solution)/shard_map/all_to_all | solution.py:97
  86.5 0.1 fusion.24
  86.5 0.2 reduce_window_sum.11
  86.7 0.2 select_reduce_fusion
  86.9 15.4 %all-to-all-done = bf16[8,64,256]{2,1,0:T(8,128)(2,1)S(1)} async-done(((bf16[8,64,256]{2,1,0:T(8,128)(2,1)}), bf16[8,64,256]{2,1,0:T(8,128)(2,1)S(1)}, u32[]{:S(2)}, u32[]{:S(2)}) %all-to-all-start) | async-done | bytes 262176 | tf_op jit(solution)/shard_map/all_to_all | solution.py:97
  102.3 53.7 %all-gather.9.cloned.1.call-done = bf16[2048,2048]{1,0:T(8,128)(2,1)} async-done(((bf16[256,2048]{1,0:T(8,128)(2,1)}), bf16[2048,2048]{1,0:T(8,128)(2,1)}) %all-gather.9.cloned.1.call-update) | async-done | bytes 8388624 | tf_op jit(solution)/shard_map/all_gather | solution.py:100
  156.0 5.1 %multiply_reduce_fusion.1 = (f32[64]{0:T(128)S(1)}, f32[64,2048]{1,0:T(8,128)S(1)}) fusion(bf16[64,2048]{1,0:T(8,128)(2,1)S(1)} %bitcast.63, bf16[2048,2048]{1,0:T(8,128)(2,1)} %all-gather.9.cloned.1.call-done, bf16[64,2048]{1,0:T(8,128)(2,1)S(1)} %copy-done.1), kind=kOutput, calls=%fused_computation.35 | convolution fusion | flops 537657280 | bytes 9437440 | tf_op jit(solution)/shard_map/dot_general | solution.py:98
  161.1 0.1 multiply_convert_fusion.1
  161.3 0.3 broadcast_in_dim.55
  161.6 0.2 reshape.139
  161.8 0.4 convolution_convert_fusion.1
  162.1 15.3 %all_to_all.29 = bf16[4,48,2048]{2,1,0:T(8,128)(2,1)} all-to-all(bf16[4,48,2048]{2,1,0:T(8,128)(2,1)S(1)} %bitcast.62), channel_id=1, replica_groups=mesh['sp'=4,'tp'=8] {'sp'}, dimensions={0} | all-to-all | bytes 1572864 | tf_op jit(solution)/shard_map/all_to_all | solution.py:121
  177.5 61.7 %all-gather.11.cloned.1.call-done = bf16[1536,2048]{1,0:T(8,128)(2,1)} async-done(((bf16[192,2048]{1,0:T(8,128)(2,1)}), bf16[1536,2048]{1,0:T(8,128)(2,1)}) %all-gather.11.cloned.1.call-update) | async-done | bytes 6291472 | tf_op jit(solution)/shard_map/all_gather | solution.py:123
  239.3 11.4 %fusion.18 = f32[1536,896]{1,0:T(8,128)} fusion(bf16[1536,2048]{1,0:T(8,128)(2,1)} %all-gather.11.cloned.1.call-done, bf16[1,2048,896]{2,1,0:T(8,128)(2,1)} %param.23), kind=kOutput, calls=%fused_computation.25 | convolution fusion | flops 5637144576 | bytes 15466496 | tf_op jit(solution)/shard_map/dot_general | solution.py:124
  250.6 20.1 %convolution_convert_fusion = bf16[1536,2048]{1,0:T(8,128)(2,1)} fusion(bf16[1,896,2048]{2,1,0:T(8,128)(2,1)} %param.25, f32[1536,896]{1,0:T(8,128)} %fusion.18, bf16[1536,2048]{1,0:T(8,128)(2,1)} %all-gather.11.cloned.1.call-done, bf16[1,2048,896]{2,1,0:T(8,128)(2,1)} %param.24), kind=kOutput, calls=%fused_computation.21 | convolution fusion | flops 11285692416 | bytes 25427968 | tf_op jit(solution)/shard_map/dot_general | solution.py:128
  270.7 68.5 %reduce-scatter.2.cloned.1.call-done = bf16[192,2048]{1,0:T(8,128)(2,1)} async-done(((bf16[1536,2048]{1,0:T(8,128)(2,1)}), bf16[192,2048]{1,0:T(8,128)(2,1)}) %reduce-scatter.2.cloned.1.call-update) | async-done | bytes 786448 | tf_op jit(solution)/shard_map/reduce_scatter | solution.py:127
  339.2 3.7 %all-to-all-start.2 = ((bf16[4,48,2048]{2,1,0:T(8,128)(2,1)}), bf16[4,48,2048]{2,1,0:T(8,128)(2,1)S(1)}, u32[]{:S(2)}, u32[]{:S(2)}) async-start(bf16[4,48,2048]{2,1,0:T(8,128)(2,1)} %bitcast.67), calls=%async_computation.3 | async-start | bytes 1572864 | tf_op jit(solution)/shard_map/all_to_all | solution.py:134
  342.9 0.1 copy.33
  343.0 0.1 mul.106
  343.2 0.1 copy.34
  343.3 8.7 %all-to-all-done.2 = bf16[4,48,2048]{2,1,0:T(8,128)(2,1)S(1)} async-done(((bf16[4,48,2048]{2,1,0:T(8,128)(2,1)}), bf16[4,48,2048]{2,1,0:T(8,128)(2,1)S(1)}, u32[]{:S(2)}, u32[]{:S(2)}) %all-to-all-start.2) | async-done | bytes 786464 | tf_op jit(solution)/shard_map/all_to_all | solution.py:134
  352.0 0.9 gather_fusion
  352.9 0.7 reshape.144
  353.6 1.5 multiply_reduce_fusion
  355.1 0.8 add_convert_fusion
  (36 shorter events, 0.4 us)
Async XLA Ops:
  6.5 61.8 %copy-start = (f32[512,4]{0,1:T(4,128)S(1)}, f32[512,4]{0,1:T(4,128)}, u32[]{:S(2)}) copy-start(f32[512,4]{0,1:T(4,128)} %param.20) | copy-start | bytes 24580
  6.5 31.9 %all-gather.5.cloned.1.call-start = ((), (), s32[]{:S(2)}) async-start(), calls=%async_computation.4 | async-start | bytes 1310720 | tf_op jit(solution)/shard_map/all_gather | solution.py:69
  7.3 59.5 %all-gather.7.cloned.1.call-start = ((), (), s32[]{:S(2)}) async-start(), calls=%async_computation.5 | async-start | bytes 1310720 | tf_op jit(solution)/shard_map/all_gather | solution.py:70
  8.0 148.0 %all-gather.9.cloned.1.call-start = ((), (), s32[]{:S(2)}) async-start(), calls=%async_computation.6 | async-start | bytes 9437184 | tf_op jit(solution)/shard_map/all_gather | solution.py:100
  68.4 87.6 %copy-start.1 = (bf16[64,2048]{1,0:T(8,128)(2,1)S(1)}, bf16[64,2048]{1,0:T(8,128)(2,1)}, u32[]{:S(2)}) copy-start(bf16[64,2048]{1,0:T(8,128)(2,1)} %param.16) | copy-start | bytes 786436
  81.8 20.5 %all-to-all-start = ((bf16[8,64,256]{2,1,0:T(8,128)(2,1)}), bf16[8,64,256]{2,1,0:T(8,128)(2,1)S(1)}, u32[]{:S(2)}, u32[]{:S(2)}) async-start(bf16[8,64,256]{2,1,0:T(8,128)(2,1)} %copy.30), calls=%async_computation | async-start | bytes 524288 | tf_op jit(solution)/shard_map/all_to_all | solution.py:97
  86.4 152.9 %all-gather.11.cloned.1.call-start = ((), (), s32[]{:S(2)}) async-start(), calls=%async_computation.7 | async-start | bytes 7077888 | tf_op jit(solution)/shard_map/all_gather | solution.py:123
  156.0 5.1 %copy-start.2 = (f32[2048]{0:T(1024)S(1)}, f32[2048]{0:T(1024)}, u32[]{:S(2)}) copy-start(f32[2048]{0:T(1024)} %param.22) | copy-start | bytes 24580
  177.5 161.8 %reduce-scatter.2.cloned.1.call-start = ((), (), s32[]{:S(2)}) async-start(), calls=%async_computation.8 | async-start | bytes 7077888 | tf_op jit(solution)/shard_map/reduce_scatter | solution.py:127
  270.7 72.2 %copy-start.3 = (s32[64,2]{0,1:T(2,128)S(1)}, s32[64,2]{0,1:T(2,128)}, u32[]{:S(2)}) copy-start(s32[64,2]{0,1:T(2,128)} %param.26) | copy-start | bytes 1540
  270.7 72.5 %copy-start.4 = (f32[64,2]{0,1:T(2,128)S(1)}, f32[64,2]{0,1:T(2,128)}, u32[]{:S(2)}) copy-start(f32[64,2]{0,1:T(2,128)} %param.27) | copy-start | bytes 1540
  339.2 12.8 %all-to-all-start.2 = ((bf16[4,48,2048]{2,1,0:T(8,128)(2,1)}), bf16[4,48,2048]{2,1,0:T(8,128)(2,1)S(1)}, u32[]{:S(2)}, u32[]{:S(2)}) async-start(bf16[4,48,2048]{2,1,0:T(8,128)(2,1)} %bitcast.67), calls=%async_computation.3 | async-start | bytes 1572864 | tf_op jit(solution)/shard_map/all_to_all | solution.py:134
Sparse Core Ops, SparseCore 0:
  9.2 29.2 all-gather.4
  40.3 26.4 all-gather.6
  68.4 87.5 all-gather.8
  177.6 61.6 all-gather.10
  270.8 68.3 reduce-scatter.1
where the time goes:
time: 363 us; the launch traced here: 362 us
  waiting for transfers between devices  255 us (70%)
  matrix products  42.6 us (12%)
  blocking collectives  25.1 us (7%)
  between operations  13.4 us (4%)
  local copies, waits for them, and re-layouts  10.3 us (3%)
  starting transfers between devices  8.43 us (2%)
  other arithmetic  6.2 us (2%)
    reduce_scatter x1, waiting for transfers between devices, shards(): lax.psum_scatter(jnp.dot(hidden, down_weight[0], preferred_element_type=j...  68.5 us
    all_gather x1, waiting for transfers between devices, shards(): rows_in = lax.all_gather(row_block, 'tp', axis=0, tiled=True)  61.7 us
    all_gather x1, waiting for transfers between devices, shards(): lax.all_gather(out_weight, 'tp', axis=0, tiled=True)  53.7 us
    all_gather x1, waiting for transfers between devices, shards(): value_piece = lax.all_gather(value_vectors, 'sp', axis=0, tiled=True)  26.9 us
    dot_general x1, matrix products, shards(): jnp.dot(hidden, down_weight[0], preferred_element_type=jnp.float32)  20.1 us
    all_gather x1, waiting for transfers between devices, shards(): key_piece = lax.all_gather(key_vectors, 'sp', axis=0, tiled=True)  17.9 us
    all_to_all x1, waiting for transfers between devices, shards(): lax.all_to_all(attended, 'tp', split_axis=0, concat_axis=1, tiled=True)  15.4 us
    all_to_all x1, blocking collectives, shards(): lax.all_to_all(dispatch, 'sp', split_axis=0, concat_axis=0, tiled=True)  15.3 us
  transfers between devices with their start and end apart: 7, of which 7 were waited for; matrix products, arithmetic and copies ran while one was open for 5% of the time, Pallas kernels for 0%

commit v1 on v0

--- a/solution.py
+++ b/solution.py
@@ -5,6 +5,18 @@
 from jax.sharding import PartitionSpec as P
 
 NEG_LARGE = -1e30
+
+
+def collect(x, axis, dim):
+    ways, here = (lax.axis_size(axis), lax.axis_index(axis))
+    grown, reach = (x, 1)
+    while reach < ways:
+        theirs = lax.ppermute(grown, axis, [(d, d ^ reach) for d in range(ways)])
+        mine_first = jnp.concatenate([grown, theirs], axis=dim)
+        theirs_first = jnp.concatenate([theirs, grown], axis=dim)
+        grown = jnp.where(here & reach == 0, mine_first, theirs_first)
+        reach = 2 * reach
+    return grown
 
 
 def shards(
@@ -96,9 +108,7 @@
     model_width = tokens.shape[1]
     token_rows = lax.all_to_all(attended, "tp", split_axis=0, concat_axis=1, tiled=True)
     projected = jnp.dot(
-        token_rows,
-        lax.all_gather(out_weight, "tp", axis=0, tiled=True),
-        preferred_element_type=jnp.float32,
+        token_rows, collect(out_weight, "tp", 0), preferred_element_type=jnp.float32
     )
     stream_wide = (tokens.astype(jnp.float32) + projected).astype(jnp.bfloat16).astype(jnp.float32)
     inverse = lax.rsqrt(jnp.mean(stream_wide * stream_wide, axis=1, keepdims=True) + 1e-05)

time: 363 us -> 466 us (1.28)
  waiting for transfers between devices: 255 us -> 347 us
  other arithmetic: 6.2 us -> 13.7 us
  starting transfers between devices: 8.43 us -> 14.8 us
    all_to_all x1, waiting for transfers between devices: 15.4 us -> 112 us  [shards(): lax.all_to_all(attended, 'tp', split_axis=0, concat_axis=1, tiled=True)]
    all_gather x1 -> x0, waiting for transfers between devices: 53.7 us -> none  [shards(): lax.all_gather(out_weight, 'tp', axis=0, tiled=True)]
    ppermute x0 -> x3, waiting for transfers between devices: none -> 48.5 us  [collect(): theirs = lax.ppermute(grown, axis, [(d, d ^ reach) for d in range(ways)])]
    select_n x0 -> x2, other arithmetic: none -> 7.51 us  [collect(): grown = jnp.where(here & reach == 0, mine_first, theirs_first)]
    ppermute x0 -> x3, starting transfers between devices: none -> 6.24 us  [collect(): theirs = lax.ppermute(grown, axis, [(d, d ^ reach) for d in range(ways)])]
  transfers between devices with their start and end apart: 7 -> 9, of which waited for: 7 -> 8; matrix products, arithmetic and copies ran while one was open for 5% -> 3% of each run, Pallas kernels for 0% -> 0%
where the time goes in v1:
time: 466 us
  waiting for transfers between devices  347 us (74%)
  matrix products  44.7 us (10%)
  blocking collectives  22.7 us (5%)
  starting transfers between devices  14.8 us (3%)
  other arithmetic  13.7 us (3%)
  between operations  13.4 us (3%)
  local copies, waits for them, and re-layouts  8.5 us (2%)
    all_to_all x1, waiting for transfers between devices, shards(): lax.all_to_all(attended, 'tp', split_axis=0, concat_axis=1, tiled=True)  112 us
    reduce_scatter x1, waiting for transfers between devices, shards(): lax.psum_scatter(jnp.dot(hidden, down_weight[0], preferred_element_type=j...  68.5 us
    all_gather x1, waiting for transfers between devices, shards(): rows_in = lax.all_gather(row_block, 'tp', axis=0, tiled=True)  65 us
    ppermute x3, waiting for transfers between devices, collect(): theirs = lax.ppermute(grown, axis, [(d, d ^ reach) for d in range(ways)])  48.5 us
    all_gather x1, waiting for transfers between devices, shards(): value_piece = lax.all_gather(value_vectors, 'sp', axis=0, tiled=True)  26.9 us
    dot_general x1, matrix products, shards(): jnp.dot(hidden, down_weight[0], preferred_element_type=jnp.float32)  20.1 us
    all_gather x1, waiting for transfers between devices, shards(): key_piece = lax.all_gather(key_vectors, 'sp', axis=0, tiled=True)  16.5 us
    all_to_all x1, blocking collectives, shards(): lax.all_to_all(dispatch, 'sp', split_axis=0, concat_axis=0, tiled=True)  14.5 us
  transfers between devices with their start and end apart: 9, of which 8 were waited for; matrix products, arithmetic and copies ran while one was open for 3% of the time, Pallas kernels for 0%

profile of v1, /device:TPU:0, one launch (start us, length us, event | category | flops | bytes accessed | tf_op | source)
XLA Modules:
  0.0 465.7 jit_solution(7201131801019771721)
XLA Ops:
  6.5 0.5 collective-permute-start
  7.0 2.5 collective-permute-done
  9.5 2.4 maximum_select_fusion.9
  11.9 3.0 collective-permute-start.1
  14.9 46.0 %collective-permute-done.1 = bf16[512,2048]{1,0:T(8,128)(2,1)} collective-permute-done((bf16[512,2048]{1,0:T(8,128)(2,1)S(1)}, bf16[512,2048]{1,0:T(8,128)(2,1)}, u32[]{:S(2)}, u32[]{:S(2)}) %collective-permute-start.1) | collective-permute-done | bytes 2097184 | tf_op jit(solution)/shard_map/ppermute | solution.py:14
  61.0 5.1 %maximum_select_fusion.2 = bf16[1024,2048]{1,0:T(8,128)(2,1)} fusion(bf16[512,2048]{1,0:T(8,128)(2,1)} %collective-permute-done.1, bf16[512,2048]{1,0:T(8,128)(2,1)S(1)} %maximum_select_fusion.9, pred[]{:T(512)S(6)} %eq.36), kind=kLoop, calls=%fused_computation.31 | loop fusion | flops 18874368 | bytes 8388609 | tf_op jit(solution)/shard_map/jit(_where)/select_n | solution.py:17
  66.1 2.8 collective-permute-start.2
  68.9 0.7 all-gather.6.cloned.1.call-update
  69.6 0.1 copy.27
  69.9 0.1 reshape.138
  70.0 8.2 %all_gather.13 = f32[2048,4]{0,1:T(4,128)S(1)} all-gather(f32[512,4]{0,1:T(4,128)S(1)} %copy-done), channel_id=1, replica_groups=mesh['sp'=4,'tp'=8] {'sp'}, dimensions={0}, use_global_device_ids=true | all-gather | bytes 40960 | tf_op jit(solution)/shard_map/all_gather | solution.py:46
  78.2 16.5 %all-gather.4.cloned.1.call-done = bf16[2048,256]{1,0:T(8,128)(2,1)} async-done(((bf16[512,256]{1,0:T(8,128)(2,1)}), bf16[2048,256]{1,0:T(8,128)(2,1)}) %all-gather.4.cloned.1.call-update) | async-done | bytes 1048592 | tf_op jit(solution)/shard_map/all_gather | solution.py:81
  94.7 1.5 copy.28
  96.2 26.9 %all-gather.6.cloned.1.call-done = bf16[2048,256]{1,0:T(8,128)(2,1)} async-done(((bf16[512,256]{1,0:T(8,128)(2,1)}), bf16[2048,256]{1,0:T(8,128)(2,1)}) %all-gather.6.cloned.1.call-update) | async-done | bytes 1048592 | tf_op jit(solution)/shard_map/all_gather | solution.py:82
  123.1 1.5 copy.29
  124.7 11.5 %while.15 = (s32[]{:T(128)}, f32[4,512]{1,0:T(4,128)S(1)}, f32[4,512]{1,0:T(4,128)S(1)}, f32[4,512,64]{1,2,0:T(8,128)S(1)}, s32[2]{0:T(128)S(1)}, /*index=5*/s32...) while((s32[]{:T(128)}, f32[4,512]{1,0:T(4,128)S(1)}, ...), condition=%wide.region_5.6_spmd.clone, body=%wide.region_0.5_spmd.clone.sunk | while | flops 577508864 | bytes 31973756 | solution.py:101
  124.7 0.6 dynamic_slice.31
  125.9 9.2 %conditional.3 = ((f32[4,512]{1,0:T(4,128)S(1)}, f32[4,512]{1,0:T(4,128)S(1)}, f32[4,512,64]{1,2,0:T(8,128)S(1)})) conditional(s32[]{:T(128)} %convert_element_type.83, (f32[4,512]{1,0:T(4,128)S(1)}, f32[4,512]{1,0:T(4,128)S(1)}, f32[4,512,64]{1,2,0:T(8,128)S(1)}) %tuple.42, (s32[]{:T(128)}, s32[]{:T(128)}, bf16[2,1024,256]{1,2,0:T(8,128)(2,1)S(1)}, ...), branch_computations={%region_1.1_spmd, %region_2.4_spmd} | conditional | flops 577508864 | bytes 31971410 | solution.py:99
  126.0 0.4 broadcast_compare_fusion
  126.4 2.5 fusion.4
  129.0 2.9 fusion.3
  131.9 3.1 fusion.8
  135.1 0.6 dynamic_slice.31
  136.3 0.3 all_to_all.20
  136.6 1.0 copy.30
  137.6 4.6 all-to-all-start
  142.2 0.2 all-gather.8.cloned.1.call-start
  142.5 0.2 reduce_window_sum.11
  142.7 0.2 select_reduce_fusion
  142.9 111.8 %all-to-all-done = bf16[8,64,256]{2,1,0:T(8,128)(2,1)S(1)} async-done(((bf16[8,64,256]{2,1,0:T(8,128)(2,1)}), bf16[8,64,256]{2,1,0:T(8,128)(2,1)S(1)}, u32[]{:S(2)}, u32[]{:S(2)}) %all-to-all-start) | async-done | bytes 262176 | tf_op jit(solution)/shard_map/all_to_all | solution.py:109
  254.8 7.3 %multiply_reduce_fusion.1 = (f32[64]{0:T(128)S(1)}, f32[64,2048]{1,0:T(8,128)S(1)}) fusion(bf16[64,2048]{1,0:T(8,128)(2,1)S(1)} %bitcast.68, bf16[1024,2048]{1,0:T(8,128)(2,1)} %collective-permute-done.2, bf16[1024,2048]{1,0:T(8,128)(2,1)} %maximum_select_fusion.2, pred[]{:T(512)S(6)} %eq.35, bf16[64,2048]{1,0:T(8,128)(2,1)S(1)} %copy-done.5), kind=kOutput, calls=%fused_computation.45 | convolution fusion | flops 575406016 | bytes 9437441 | tf_op jit(solution)/shard_map/dot_general | solution.py:110
  262.1 0.1 multiply_convert_fusion.1
  262.2 0.3 broadcast_in_dim.55
  262.5 0.2 reshape.139
  262.7 0.4 convolution_convert_fusion.1
  263.1 14.5 %all_to_all.29 = bf16[4,48,2048]{2,1,0:T(8,128)(2,1)} all-to-all(bf16[4,48,2048]{2,1,0:T(8,128)(2,1)S(1)} %bitcast.61), channel_id=1, replica_groups=mesh['sp'=4,'tp'=8] {'sp'}, dimensions={0} | all-to-all | bytes 1572864 | tf_op jit(solution)/shard_map/all_to_all | solution.py:131
  277.6 65.0 %all-gather.8.cloned.1.call-done = bf16[1536,2048]{1,0:T(8,128)(2,1)} async-done(((bf16[192,2048]{1,0:T(8,128)(2,1)}), bf16[1536,2048]{1,0:T(8,128)(2,1)}) %all-gather.8.cloned.1.call-update) | async-done | bytes 6291472 | tf_op jit(solution)/shard_map/all_gather | solution.py:133
  342.6 11.3 %fusion.25 = f32[1536,896]{1,0:T(8,128)} fusion(bf16[1536,2048]{1,0:T(8,128)(2,1)} %all-gather.8.cloned.1.call-done, bf16[1,2048,896]{2,1,0:T(8,128)(2,1)} %param.23), kind=kOutput, calls=%fused_computation.34 | convolution fusion | flops 5637144576 | bytes 15466496 | tf_op jit(solution)/shard_map/dot_general | solution.py:134
  353.9 20.1 %convolution_convert_fusion = bf16[1536,2048]{1,0:T(8,128)(2,1)} fusion(bf16[1,896,2048]{2,1,0:T(8,128)(2,1)} %param.25, f32[1536,896]{1,0:T(8,128)} %fusion.25, bf16[1536,2048]{1,0:T(8,128)(2,1)} %all-gather.8.cloned.1.call-done, bf16[1,2048,896]{2,1,0:T(8,128)(2,1)} %param.24), kind=kOutput, calls=%fused_computation.29 | convolution fusion | flops 11285692416 | bytes 25427968 | tf_op jit(solution)/shard_map/dot_general | solution.py:138
  374.0 68.5 %reduce-scatter.2.cloned.1.call-done = bf16[192,2048]{1,0:T(8,128)(2,1)} async-done(((bf16[1536,2048]{1,0:T(8,128)(2,1)}), bf16[192,2048]{1,0:T(8,128)(2,1)}) %reduce-scatter.2.cloned.1.call-update) | async-done | bytes 786448 | tf_op jit(solution)/shard_map/reduce_scatter | solution.py:137
  442.6 3.6 all-to-all-start.2
  446.2 0.1 copy.33
  446.3 0.1 mul.106
  446.6 8.7 %all-to-all-done.2 = bf16[4,48,2048]{2,1,0:T(8,128)(2,1)S(1)} async-done(((bf16[4,48,2048]{2,1,0:T(8,128)(2,1)}), bf16[4,48,2048]{2,1,0:T(8,128)(2,1)S(1)}, u32[]{:S(2)}, u32[]{:S(2)}) %all-to-all-start.2) | async-done | bytes 786464 | tf_op jit(solution)/shard_map/all_to_all | solution.py:144
  455.3 0.9 gather_fusion
  456.2 0.7 reshape.144
  456.9 1.5 multiply_reduce_fusion
  458.4 0.8 add_convert_fusion
  (43 shorter events, 0.8 us)
Async XLA Ops:
  6.5 88.2 %all-gather.4.cloned.1.call-start = ((), (), s32[]{:S(2)}) async-start(), calls=%async_computation.4 | async-start | bytes 1310720 | tf_op jit(solution)/shard_map/all_gather | solution.py:81
  6.5 3.0 collective-permute-start
  7.0 62.6 %copy-start.1 = (bf16[512,256]{1,0:T(8,128)(2,1)S(1)}, bf16[512,256]{1,0:T(8,128)(2,1)}, u32[]{:S(2)}) copy-start(bf16[512,256]{1,0:T(8,128)(2,1)} %param.17) | copy-start | bytes 786436
  7.0 62.7 %copy-start.3 = (s32[64,2]{0,1:T(2,128)S(1)}, s32[64,2]{0,1:T(2,128)}, u32[]{:S(2)}) copy-start(s32[64,2]{0,1:T(2,128)} %param.26) | copy-start | bytes 1540
  7.0 63.0 %copy-start = (f32[512,4]{0,1:T(4,128)S(1)}, f32[512,4]{0,1:T(4,128)}, u32[]{:S(2)}) copy-start(f32[512,4]{0,1:T(4,128)} %param.20) | copy-start | bytes 24580
  11.9 49.0 %collective-permute-start.1 = (bf16[512,2048]{1,0:T(8,128)(2,1)S(1)}, bf16[512,2048]{1,0:T(8,128)(2,1)}, u32[]{:S(2)}, u32[]{:S(2)}) collective-permute-start(bf16[512,2048]{1,0:T(8,128)(2,1)S(1)} %maximum_select_fusion.9), channel_id=1, source_target_pairs={{0,2},{1,3},{2,0},{3,1},{4,6},{5,7},{6,4},{7,5},{8,10},{9,11},{10,... | collective-permute-start | bytes 6291464 | tf_op jit(solution)/shard_map/ppermute | solution.py:14
  66.1 188.7 %collective-permute-start.2 = (bf16[1024,2048]{1,0:T(8,128)(2,1)}, bf16[1024,2048]{1,0:T(8,128)(2,1)}, u32[]{:S(2)}, u32[]{:S(2)}) collective-permute-start(bf16[1024,2048]{1,0:T(8,128)(2,1)} %maximum_select_fusion.2), channel_id=1, source_target_pairs={{0,4},{1,5},{2,6},{3,7},{4,0},{5,1},{6,2},{7,3},{8,12},{9,13},{10,... | collective-permute-start | bytes 12582920 | tf_op jit(solution)/shard_map/ppermute | solution.py:14
  68.9 54.2 %all-gather.6.cloned.1.call-start = ((), (), s32[]{:S(2)}) async-start(), calls=%async_computation.5 | async-start | bytes 1310720 | tf_op jit(solution)/shard_map/all_gather | solution.py:82
  124.7 130.1 %copy-start.5 = (bf16[64,2048]{1,0:T(8,128)(2,1)S(1)}, bf16[64,2048]{1,0:T(8,128)(2,1)}, u32[]{:S(2)}) copy-start(bf16[64,2048]{1,0:T(8,128)(2,1)} %param.16) | copy-start | bytes 786436
  137.6 117.1 %all-to-all-start = ((bf16[8,64,256]{2,1,0:T(8,128)(2,1)}), bf16[8,64,256]{2,1,0:T(8,128)(2,1)S(1)}, u32[]{:S(2)}, u32[]{:S(2)}) async-start(bf16[8,64,256]{2,1,0:T(8,128)(2,1)} %copy.30), calls=%async_computation | async-start | bytes 524288 | tf_op jit(solution)/shard_map/all_to_all | solution.py:109
  142.2 200.3 %all-gather.8.cloned.1.call-start = ((), (), s32[]{:S(2)}) async-start(), calls=%async_computation.6 | async-start | bytes 7077888 | tf_op jit(solution)/shard_map/all_gather | solution.py:133
  254.8 7.3 %copy-start.2 = (f32[2048]{0:T(1024)S(1)}, f32[2048]{0:T(1024)}, u32[]{:S(2)}) copy-start(f32[2048]{0:T(1024)} %param.22) | copy-start | bytes 24580
  277.6 165.0 %reduce-scatter.2.cloned.1.call-start = ((), (), s32[]{:S(2)}) async-start(), calls=%async_computation.7 | async-start | bytes 7077888 | tf_op jit(solution)/shard_map/reduce_scatter | solution.py:137
  374.0 72.4 %copy-start.4 = (f32[64,2]{0,1:T(2,128)S(1)}, f32[64,2]{0,1:T(2,128)}, u32[]{:S(2)}) copy-start(f32[64,2]{0,1:T(2,128)} %param.27) | copy-start | bytes 1540
  442.6 12.7 %all-to-all-start.2 = ((bf16[4,48,2048]{2,1,0:T(8,128)(2,1)}), bf16[4,48,2048]{2,1,0:T(8,128)(2,1)S(1)}, u32[]{:S(2)}, u32[]{:S(2)}) async-start(bf16[4,48,2048]{2,1,0:T(8,128)(2,1)} %bitcast.65), calls=%async_computation.3 | async-start | bytes 1572864 | tf_op jit(solution)/shard_map/all_to_all | solution.py:144
Sparse Core Ops, SparseCore 0:
  69.0 25.7 all-gather.3
  96.6 26.4 all-gather.5
  277.7 64.8 all-gather.7
  374.1 68.3 reduce-scatter.1
